TPU v7x, 32 devices: a whole 2x2x4 slice. The times are simulated.
32 devices in a mesh: ep: 8 (over z, x), tp: 4 (over y, core).
Axes of the slice: x: 2, y: 2, z: 4, core: 2. Of those that a mesh axis runs over, the one named last changes fastest.
Arguments:
- tokens: bfloat16 [32, 2048], P('ep'), may hold values from -6 to 6
- norm_gain: bfloat16 [2048], replicated, may hold values from 0.099609375 to 1.8984375
- in_weight: bfloat16 [2048, 1024], P(None, 'tp'), may hold values from -0.125 to 0.125
- decay_rate: float32 [64, 64], P('tp'), may hold values from 0.05 to 1
- frequency: float32 [64, 64], P('tp'), may hold values from -3 to 3
- log_step: float32 [64], P('tp'), may hold values from -2.3 to 0.7
- input_real: float32 [64, 64, 16], P('tp'), may hold values from -1.75 to 1.75
- input_imag: float32 [64, 64, 16], P('tp'), may hold values from -1.75 to 1.75
- output_real: float32 [64, 16, 64], P('tp'), may hold values from -0.5 to 0.5
- output_imag: float32 [64, 16, 64], P('tp'), may hold values from -0.5 to 0.5
- skip_gain: float32 [1024], P('tp'), may hold values from -3 to 3
- state_real: float32 [32, 64, 64], P('ep', 'tp'), may hold values from -6 to 6
- state_imag: float32 [32, 64, 64], P('ep', 'tp'), may hold values from -6 to 6
- out_weight: bfloat16 [1024, 2048], P('tp'), may hold values from -0.1875 to 0.1875
- ffn_gain: bfloat16 [2048], replicated, may hold values from 0.099609375 to 1.8984375
- expert_ids: int32 [32, 2], replicated, may hold values from 0 to 7, all different within a row; in each aligned block of 4 rows (0 to 3, 4 to 7, ...) at most 2 rows name the same one
- route_weights: float32 [32, 2], P('ep'), may hold values from 0.2 to 1
- gate_weight: bfloat16 [2048, 65536], P(None, ('ep', 'tp')), may hold values from -0.125 to 0.125
- up_weight: bfloat16 [2048, 65536], P(None, ('ep', 'tp')), may hold values from -0.125 to 0.125
- down_weight: bfloat16 [65536, 2048], P('ep', 'tp'), may hold values from -0.0625 to 0.0625
Outputs:
- mixed: bfloat16 [32, 2048], P('ep', 'tp')
- new_real: float32 [32, 64, 64], P('ep', 'tp')
- new_imag: float32 [32, 64, 64], P('ep', 'tp')
Inputs may be any that keep to these rules, and one draw needn't show every extreme that they name: `expert_ids`: the 2 experts of a row differ. In each aligned block of 4 rows (the rows of one index of ep) no expert is named by more than 2 rows, and in some blocks one expert is named by exactly 2 rows.
All inputs are finite; a program needn't handle non-finite values.
Results may differ from a plain program's by a relative error of at most 0.007.
Values may be sent and summed in bfloat16 or wider, within the bound.
A program may use at most 64 MiB of HBM per device.

v0:
```python
import jax
import jax.numpy as jnp
from jax import lax
from jax.sharding import PartitionSpec as P

EXPERTS = 8
EPSILON = 1e-06


def rms_scale(values, gain):
    floats = values.astype(jnp.float32)
    return (
        floats
        * lax.rsqrt(jnp.mean(floats * floats, axis=-1, keepdims=True) + EPSILON)
        * gain.astype(jnp.float32)
    )


def discretize(decay_rate, frequency, log_step, input_real, input_imag):
    step_size = jnp.exp(log_step)[:, None]
    lam_real = -decay_rate
    magnitude = jnp.exp(lam_real * step_size)
    turned = frequency * step_size
    bar_real = magnitude * jnp.cos(turned)
    bar_imag = magnitude * jnp.sin(turned)
    denom = lam_real * lam_real + frequency * frequency
    minus_one = bar_real - 1.0
    factor_real = (minus_one * lam_real + bar_imag * frequency) / denom
    factor_imag = (bar_imag * lam_real - minus_one * frequency) / denom
    b_real = factor_real[..., None] * input_real - factor_imag[..., None] * input_imag
    b_imag = factor_real[..., None] * input_imag + factor_imag[..., None] * input_real
    return (bar_real, bar_imag, b_real, b_imag)


def state_update(
    projected,
    state_real,
    state_imag,
    decay_rate,
    frequency,
    log_step,
    input_real,
    input_imag,
    output_real,
    output_imag,
    skip_gain,
):
    bar_real, bar_imag, b_real, b_imag = discretize(
        decay_rate, frequency, log_step, input_real, input_imag
    )
    count, groups, _ = state_real.shape
    high = lax.Precision.HIGHEST
    grouped = projected.astype(jnp.float32).reshape(count, groups, -1)
    drive_real = jnp.einsum("sgp,gnp->sgn", grouped, b_real, precision=high)
    drive_imag = jnp.einsum("sgp,gnp->sgn", grouped, b_imag, precision=high)
    new_real = bar_real * state_real - bar_imag * state_imag + drive_real
    new_imag = bar_real * state_imag + bar_imag * state_real + drive_imag
    readout = jnp.einsum("sgn,gpn->sgp", new_real, output_real, precision=high) - jnp.einsum(
        "sgn,gpn->sgp", new_imag, output_imag, precision=high
    )
    readout = readout.reshape(count, -1) + skip_gain * grouped.reshape(count, -1)
    return (jax.nn.gelu(readout).astype(jnp.bfloat16), new_real, new_imag)


def slot_table(own_ids, own_weights, slot_count):
    expert_range = jnp.arange(EXPERTS, dtype=jnp.int32)
    onehot = (own_ids[:, :, None] == expert_range).astype(jnp.int32)
    flat = onehot.reshape(-1, EXPERTS)
    before = (jnp.cumsum(flat, axis=0) - flat).reshape(onehot.shape)
    slots = jnp.arange(slot_count, dtype=jnp.int32)
    match = (before[..., None] == slots) & (onehot[..., None] > 0)
    table = jnp.sum(jnp.where(match, own_weights[:, :, None, None], 0.0), axis=1)
    return jnp.transpose(table, (1, 2, 0))


def shards(
    tokens,
    norm_gain,
    in_weight,
    decay_rate,
    frequency,
    log_step,
    input_real,
    input_imag,
    output_real,
    output_imag,
    skip_gain,
    state_real,
    state_imag,
    out_weight,
    ffn_gain,
    expert_ids,
    route_weights,
    gate_weight,
    up_weight,
    down_weight,
):
    normed_in = rms_scale(tokens, norm_gain).astype(jnp.bfloat16)
    projected = jnp.dot(normed_in, in_weight, preferred_element_type=jnp.float32).astype(
        jnp.bfloat16
    )
    activated, new_real, new_imag = state_update(
        projected,
        state_real,
        state_imag,
        decay_rate,
        frequency,
        log_step,
        input_real,
        input_imag,
        output_real,
        output_imag,
        skip_gain,
    )
    delta = lax.psum(jnp.dot(activated, out_weight, preferred_element_type=jnp.float32), "tp")
    hidden_state = (tokens.astype(jnp.float32) + delta).astype(jnp.bfloat16)
    normed = rms_scale(hidden_state, ffn_gain).astype(jnp.bfloat16)
    seq_count, width = normed.shape
    slot_count = seq_count // 2
    group_span = lax.axis_size("ep") // EXPERTS
    my_index = lax.axis_index("ep")
    own_ids = lax.dynamic_slice_in_dim(expert_ids, my_index * seq_count, seq_count, 0)
    unit_weights = jnp.ones(own_ids.shape, jnp.float32)
    select = slot_table(own_ids, unit_weights, slot_count)
    outgoing = jnp.einsum(
        "xcs,sd->xcd", select.astype(jnp.bfloat16), normed, preferred_element_type=jnp.float32
    ).astype(jnp.bfloat16)
    received = lax.all_to_all(
        jnp.repeat(outgoing, group_span, axis=0), "ep", split_axis=0, concat_axis=0, tiled=True
    )
    slot_rows = received.reshape(-1, width)
    gate_pre = jnp.dot(slot_rows, gate_weight, preferred_element_type=jnp.float32)
    up_pre = jnp.dot(slot_rows, up_weight, preferred_element_type=jnp.float32)
    hidden = (jax.nn.silu(gate_pre) * up_pre).astype(jnp.bfloat16)
    quarter = down_weight.shape[1]
    partial_out = jnp.dot(
        lax.all_gather(hidden, "tp", axis=1, tiled=True),
        down_weight,
        preferred_element_type=jnp.float32,
    )
    rounded = partial_out.astype(jnp.bfloat16).reshape(-1, slot_count, quarter)
    returned = lax.all_to_all(rounded, "ep", split_axis=0, concat_axis=0, tiled=True)
    summed = (
        returned.astype(jnp.float32).reshape(EXPERTS, group_span, slot_count, quarter).sum(axis=1)
    )
    weight_table = slot_table(own_ids, route_weights, slot_count)
    routed = jnp.einsum("xcs,xcd->sd", weight_table, summed, precision=lax.Precision.HIGHEST)
    residual = lax.dynamic_slice_in_dim(hidden_state, lax.axis_index("tp") * quarter, quarter, 1)
    mixed = (residual.astype(jnp.float32) + routed).astype(jnp.bfloat16)
    return (mixed, new_real, new_imag)


def solution(mesh):
    in_specs = (
        P("ep", None),
        P(),
        P(None, "tp"),
        P("tp", None),
        P("tp", None),
        P("tp"),
        P("tp", None, None),
        P("tp", None, None),
        P("tp", None, None),
        P("tp", None, None),
        P("tp"),
        P("ep", "tp", None),
        P("ep", "tp", None),
        P("tp", None),
        P(),
        P(),
        P("ep", None),
        P(None, ("ep", "tp")),
        P(None, ("ep", "tp")),
        P("ep", "tp"),
    )
    out_specs = (P("ep", "tp"), P("ep", "tp", None), P("ep", "tp", None))
    return jax.shard_map(shards, mesh=mesh, in_specs=in_specs, out_specs=out_specs, check_vma=False)
```

profile of v0, /device:TPU:0, one launch (start us, length us, event | category | flops | bytes accessed | tf_op | source)
XLA Modules:
  0.0 71.3 jit_solution(13652618909060821899)
XLA Ops:
  0.6 0.0 copy-start
  0.7 0.8 %constant_dynamic-slice_fusion = s32[4,2]{0,1:T(2,128)S(1)} fusion(s32[32,2]{0,1:T(2,128)} %param.35, s32[]{:T(128)S(6)} %select_n.14), kind=kLoop, calls=%fused_computation.78 | loop fusion | bytes 68 | tf_op jit(solution)/shard_map/dynamic_slice | solution.py:122
  1.5 0.1 copy.71
  1.6 0.1 eq.56
  1.7 0.1 fusion.42
  1.7 0.7 exp.10
  2.4 0.9 %fusion.19 = f32[4]{0:T(128)S(1)} fusion(bf16[4,2048]{1,0:T(4,128)(2,1)} %param.20), kind=kLoop, calls=%fused_computation.32 | loop fusion | flops 24572 | bytes 16400 | tf_op jit(solution)/shard_map/reduce_sum | solution.py:14
  3.3 0.7 convert_element_type.68
  4.0 1.5 %convolution_convert_fusion.2 = bf16[4,256]{1,0:T(4,128)(2,1)S(1)} fusion(bf16[2048,256]{1,0:T(8,128)(2,1)} %param.22, bf16[4,2048]{1,0:T(4,128)(2,1)} %param.20, f32[2048]{0:T(1024)S(1)} %convert_element_type.68, f32[4]{0:T(128)S(1)} %add_rsqrt_fusion.1), kind=kOutput, calls=%fused_computation.13 | convolution fusion | flops 4228096 | bytes 1075216 | tf_op jit(solution)/shard_map/dot_general | solution.py:99
  5.5 0.1 reshape.72
  5.6 0.8 %cosine_multiply_fusion = (f32[16,64]{1,0:T(8,128)S(1)}, f32[16,64]{1,0:T(8,128)S(1)}, f32[16,64]{1,0:T(8,128)S(1)}, f32[16,64]{1,0:T(8,128)S(1)}) fusion(f32[16,64]{1,0:T(8,128)} %param.24, f32[16,64]{1,0:T(8,128)} %param.23, f32[16]{0:T(128)S(1)} %exp.10), kind=kLoop, calls=%fused_computation.51 | loop fusion | flops 17408 | bytes 24640 | tf_op jit(solution)/shard_map/mul | solution.py:24
  6.4 1.2 %fusion.2 = f32[4,16,64]{2,0,1:T(4,128)S(1)} fusion(f32[16,64,16]{1,2,0:T(8,128)} %param.26, f32[16,64,16]{1,2,0:T(8,128)} %param.27, f32[16,64]{1,0:T(8,128)S(1)} %get-tuple-element.21, f32[16,64]{1,0:T(8,128)S(1)} %get-tuple-element.20, f32[4,16,64]{2,1,0:T(8,128)} %param.32, f32[4,16,64]{2,1,0:T(8,128)} %param.31, f32[16,64]{1,0:T(8,128)S(1)} %get-tuple-element.22, ...), kind=kOutput, calls=%fused_computation.6 | convolution fusion | flops 851968 | bytes 198656 | tf_op jit(solution)/shard_map/sgp,gnp->sgn/dot_general | solution.py:55
  7.6 1.2 %fusion.3 = f32[4,16,64]{2,0,1:T(4,128)S(1)} fusion(f32[16,64,16]{1,2,0:T(8,128)} %param.27, f32[16,64,16]{1,2,0:T(8,128)} %param.26, f32[16,64]{1,0:T(8,128)S(1)} %get-tuple-element.21, f32[16,64]{1,0:T(8,128)S(1)} %get-tuple-element.20, f32[4,16,64]{2,1,0:T(8,128)} %param.32, f32[4,16,64]{2,1,0:T(8,128)} %param.31, f32[16,64]{1,0:T(8,128)S(1)} %get-tuple-element.22, ...), kind=kOutput, calls=%fused_computation.8 | convolution fusion | flops 851968 | bytes 198656 | tf_op jit(solution)/shard_map/sgp,gnp->sgn/dot_general | solution.py:54
  8.8 0.1 fusion.45
  8.9 0.1 fusion.43
  9.0 0.7 convert_element_type.80
  9.7 1.2 %fusion.60 = f32[16,4,16]{2,1,0:T(4,128)S(1)} fusion(f32[4,16,64]{2,0,1:T(4,128)S(1)} %fusion.3, f32[16,16,64]{2,1,0:T(8,128)} %param.28), kind=kOutput, calls=%fused_computation.84 | convolution fusion | flops 786432 | bytes 86016 | tf_op jit(solution)/shard_map/sgn,gpn->sgp/dot_general | solution.py:58
  10.9 1.2 %fusion.1 = f32[4,16,16]{2,0,1:T(4,128)S(1)} fusion(f32[16,4,16]{2,1,0:T(4,128)S(1)} %fusion.60, f32[4,16,64]{2,0,1:T(4,128)S(1)} %fusion.2, f32[16,16,64]{2,1,0:T(8,128)} %param.29), kind=kOutput, calls=%fused_computation.4 | convolution fusion | flops 787456 | bytes 90112 | tf_op jit(solution)/shard_map/sgn,gpn->sgp/dot_general | solution.py:58
  12.1 0.1 reshape.73
  12.2 0.0 copy-done
  12.2 0.9 %fusion.46 = f32[4,2048]{1,0:T(4,128)S(1)} fusion(bf16[256,2048]{1,0:T(8,128)(2,1)S(1)} %copy-done, f32[4,256]{1,0:T(4,128)S(1)} %reshape.73, bf16[4,256]{1,0:T(4,128)(2,1)S(1)} %convolution_convert_fusion.2, f32[256]{0:T(256)} %param.30), kind=kOutput, calls=%fused_computation.69 | convolution fusion | flops 4206592 | bytes 1088512 | tf_op jit(solution)/shard_map/dot_general | solution.py:115
  13.2 12.9 %psum.7 = f32[4,2048]{1,0:T(4,128)S(1)} all-reduce(f32[4,2048]{1,0:T(4,128)S(1)} %fusion.46), channel_id=1, replica_groups=mesh['ep'=8,'tp'=4] {'tp'}, use_global_device_ids=true, to_apply=%region_1.0 | all-reduce | flops 8192 | bytes 65536 | tf_op jit(solution)/shard_map/psum | solution.py:115
  26.1 0.9 %fusion.16 = (f32[4]{0:T(128)S(1)}, bf16[4,2048]{1,0:T(4,128)(2,1)S(1)}) fusion(f32[4,2048]{1,0:T(4,128)S(1)} %psum.7, bf16[4,2048]{1,0:T(4,128)(2,1)} %param.20), kind=kLoop, calls=%fused_computation.29 | loop fusion | flops 49148 | bytes 65552 | tf_op jit(solution)/shard_map/reduce_sum | solution.py:14
  26.9 0.8 %select_reduce_fusion.1 = (f32[4,8,2]{1,0,2:T(4,128)S(1)}, bf16[4,8,2]{1,0,2:T(4,128)(2,1)S(1)}) fusion(f32[4,2]{0,1:T(2,128)} %param.36, s32[4,2,8]{2,0,1:T(4,128)S(1)} %copy.73, pred[4,2,8]{2,0,1:T(4,128)(4,1)S(1)} %copy.74), kind=kLoop, calls=%fused_computation.45 | loop fusion | flops 640 | bytes 736 | tf_op jit(solution)/shard_map/reduce_sum | solution.py:72
  27.7 0.2 convolution_convert_fusion
  27.9 0.1 copy.75
  28.0 12.5 %all_to_all.10 = bf16[8,2,2048]{2,1,0:T(2,128)(2,1)S(1)} all-to-all(bf16[8,2,2048]{2,1,0:T(2,128)(2,1)S(1)} %copy.75), channel_id=1, replica_groups=mesh['ep'=8,'tp'=4] {'ep'}, dimensions={0} | all-to-all | bytes 131072 | tf_op jit(solution)/shard_map/all_to_all | solution.py:128
  40.5 4.6 %fusion.61 = f32[16,2048]{1,0:T(8,128)S(1)} fusion(bf16[16,2048]{1,0:T(8,128)(2,1)S(1)} %reshape.74, bf16[2048,2048]{1,0:T(8,128)(2,1)} %param.37), kind=kOutput, calls=%fused_computation.85 | convolution fusion | flops 134217728 | bytes 8585216 | tf_op jit(solution)/shard_map/dot_general | solution.py:132
  45.1 4.6 %fusion = bf16[16,2048]{1,0:T(8,128)(2,1)S(1)} fusion(bf16[16,2048]{1,0:T(8,128)(2,1)S(1)} %reshape.74, bf16[2048,2048]{1,0:T(8,128)(2,1)} %param.38, f32[16,2048]{1,0:T(8,128)S(1)} %fusion.61), kind=kOutput, calls=%fused_computation.2 | convolution fusion | flops 134414336 | bytes 8650752 | tf_op jit(solution)/shard_map/dot_general | solution.py:133
  49.7 5.8 %all_gather.3 = bf16[16,8192]{1,0:T(8,128)(2,1)S(1)} all-gather(bf16[16,2048]{1,0:T(8,128)(2,1)S(1)} %fusion), channel_id=1, replica_groups=mesh['ep'=8,'tp'=4] {'tp'}, dimensions={1}, use_global_device_ids=true | all-gather | bytes 327680 | tf_op jit(solution)/shard_map/all_gather | solution.py:137
  55.5 4.6 %convolution_convert_fusion.1 = bf16[16,512]{1,0:T(8,128)(2,1)S(1)} fusion(bf16[16,8192]{1,0:T(8,128)(2,1)S(1)} %all_gather.3, bf16[8192,512]{1,0:T(8,128)(2,1)} %param.39), kind=kOutput, calls=%fused_computation.9 | convolution fusion | flops 134225920 | bytes 8667136 | tf_op jit(solution)/shard_map/dot_general | solution.py:136
  60.0 0.6 reshape.75
  60.7 3.3 %all-to-all-start.1 = ((bf16[8,2,512]{2,1,0:T(2,128)(2,1)}), bf16[8,2,512]{2,1,0:T(2,128)(2,1)S(1)}, u32[]{:S(2)}, u32[]{:S(2)}) async-start(bf16[8,2,512]{2,1,0:T(2,128)(2,1)} %reshape.75), calls=%async_computation.1 | async-start | bytes 32768 | tf_op jit(solution)/shard_map/all_to_all | solution.py:142
  64.0 0.6 copy.77
  64.6 0.6 copy.78
  65.2 5.3 %all-to-all-done.1 = bf16[8,2,512]{2,1,0:T(2,128)(2,1)S(1)} async-done(((bf16[8,2,512]{2,1,0:T(2,128)(2,1)}), bf16[8,2,512]{2,1,0:T(2,128)(2,1)S(1)}, u32[]{:S(2)}, u32[]{:S(2)}) %all-to-all-start.1) | async-done | bytes 16416 | tf_op jit(solution)/shard_map/all_to_all | solution.py:142
  70.5 0.8 %fusion.5 = bf16[4,512]{1,0:T(4,128)(2,1)} fusion(bf16[8,2,512]{2,1,0:T(2,128)(2,1)S(1)} %all-to-all-done.1, f32[4,8,2]{1,0,2:T(4,128)S(1)} %get-tuple-element.15, bf16[4,2048]{1,0:T(4,128)(2,1)S(1)} %get-tuple-element.18, s32[]{:T(128)S(6)} %select_n.13), kind=kOutput, calls=%fused_computation.12 | convolution fusion | flops 399360 | bytes 24836 | tf_op jit(solution)/shard_map/xcs,xcd->sd/dot_general | solution.py:147
  (7 shorter events, 0.1 us)
Async XLA Ops:
  0.6 11.6 %copy-start = (bf16[256,2048]{1,0:T(8,128)(2,1)S(1)}, bf16[256,2048]{1,0:T(8,128)(2,1)}, u32[]{:S(2)}) copy-start(bf16[256,2048]{1,0:T(8,128)(2,1)} %param.33) | copy-start | bytes 3145732
  60.7 9.9 %all-to-all-start.1 = ((bf16[8,2,512]{2,1,0:T(2,128)(2,1)}), bf16[8,2,512]{2,1,0:T(2,128)(2,1)S(1)}, u32[]{:S(2)}, u32[]{:S(2)}) async-start(bf16[8,2,512]{2,1,0:T(2,128)(2,1)} %reshape.75), calls=%async_computation.1 | async-start | bytes 32768 | tf_op jit(solution)/shard_map/all_to_all | solution.py:142
where the time goes:
time: 72.1 us; the launch traced here: 71.3 us
  blocking collectives  31.2 us (43%)
  matrix products  22 us (31%)
  waiting for transfers between devices  5.28 us (7%)
  other arithmetic  4.97 us (7%)
  local copies, waits for them, and re-layouts  3.84 us (5%)
  starting transfers between devices  3.33 us (5%)
  between operations  0.73 us (1%)
    psum x1, blocking collectives, shards(): lax.psum(jnp.dot(activated, out_weight, preferred_element_type=jnp.float3...  12.9 us
    all_to_all x1, blocking collectives, shards(): lax.all_to_all(jnp.repeat(outgoing, group_span, axis=0), 'ep', split_axis...  12.5 us
    all_gather x1, blocking collectives, shards(): lax.all_gather(hidden, 'tp', axis=1, tiled=True)  5.77 us
    all_to_all x1, waiting for transfers between devices, shards(): lax.all_to_all(rounded, 'ep', split_axis=0, concat_axis=0, tiled=True)  5.28 us
    dot_general x1, matrix products, shards(): up_pre = jnp.dot(slot_rows, up_weight, preferred_element_type=jnp.float32)  4.58 us
    dot_general x1, matrix products, shards(): jnp.dot(slot_rows, gate_weight, preferred_element_type=jnp.float32)  4.58 us
    dot_general x1, matrix products, shards(): jnp.dot(lax.all_gather(hidden, 'tp', axis=1, tiled=True), down_weight, pr...  4.56 us
    all_to_all x1, starting transfers between devices, shards(): lax.all_to_all(rounded, 'ep', split_axis=0, concat_axis=0, tiled=True)  3.33 us
  transfers between devices with their start and end apart: 1, of which 1 were waited for; matrix products, arithmetic and copies ran while one was open for 2% of the time, Pallas kernels for 0%

commit v1 on v0

--- a/solution.py
+++ b/solution.py
@@ -5,6 +5,12 @@
 
 EXPERTS = 8
 EPSILON = 1e-06
+
+
+def summed_here(value, name):
+    parts = lax.all_gather(value, name, axis=0, tiled=False)
+    total = parts.sum(axis=0)
+    return total
 
 
 def rms_scale(values, gain):
@@ -112,7 +118,7 @@
         output_imag,
         skip_gain,
     )
-    delta = lax.psum(jnp.dot(activated, out_weight, preferred_element_type=jnp.float32), "tp")
+    delta = summed_here(jnp.dot(activated, out_weight, preferred_element_type=jnp.float32), "tp")
     hidden_state = (tokens.astype(jnp.float32) + delta).astype(jnp.bfloat16)
     normed = rms_scale(hidden_state, ffn_gain).astype(jnp.bfloat16)
     seq_count, width = normed.shape

time: 72.1 us -> 66 us (0.915)
  blocking collectives: 31.2 us -> 25.2 us
    psum x1 -> x0, blocking collectives: 12.9 us -> none  [shards(): lax.psum(jnp.dot(activated, out_weight, preferred_element_type=jnp.float3...]
    all_gather x0 -> x1, blocking collectives: none -> 6.53 us  [summed_here(): parts = lax.all_gather(value, name, axis=0, tiled=False)]
where the time goes in v1:
time: 66 us; the launch traced here: 65.3 us
  blocking collectives  25.2 us (38%)
  matrix products  22 us (33%)
  waiting for transfers between devices  5.28 us (8%)
  other arithmetic  5 us (8%)
  local copies, waits for them, and re-layouts  3.84 us (6%)
  starting transfers between devices  3.33 us (5%)
  between operations  0.72 us (1%)
    all_to_all x1, blocking collectives, shards(): lax.all_to_all(jnp.repeat(outgoing, group_span, axis=0), 'ep', split_axis...  12.9 us
    all_gather x1, blocking collectives, summed_here(): parts = lax.all_gather(value, name, axis=0, tiled=False)  6.53 us
    all_gather x1, blocking collectives, shards(): lax.all_gather(hidden, 'tp', axis=1, tiled=True)  5.77 us
    all_to_all x1, waiting for transfers between devices, shards(): lax.all_to_all(rounded, 'ep', split_axis=0, concat_axis=0, tiled=True)  5.28 us
    dot_general x1, matrix products, shards(): up_pre = jnp.dot(slot_rows, up_weight, preferred_element_type=jnp.float32)  4.58 us
    dot_general x1, matrix products, shards(): jnp.dot(slot_rows, gate_weight, preferred_element_type=jnp.float32)  4.58 us
    dot_general x1, matrix products, shards(): jnp.dot(lax.all_gather(hidden, 'tp', axis=1, tiled=True), down_weight, pr...  4.56 us
    all_to_all x1, starting transfers between devices, shards(): lax.all_to_all(rounded, 'ep', split_axis=0, concat_axis=0, tiled=True)  3.33 us
  transfers between devices with their start and end apart: 1, of which 1 were waited for; matrix products, arithmetic and copies ran while one was open for 2% of the time, Pallas kernels for 0%

profile of v1, /device:TPU:0, one launch (start us, length us, event | category | flops | bytes accessed | tf_op | source)
XLA Modules:
  0.0 65.3 jit_solution(859107882188646898)
XLA Ops:
  0.6 0.0 copy-start
  0.7 0.8 %constant_dynamic-slice_fusion = s32[4,2]{0,1:T(2,128)S(1)} fusion(s32[32,2]{0,1:T(2,128)} %param.35, s32[]{:T(128)S(6)} %select_n.14), kind=kLoop, calls=%fused_computation.78 | loop fusion | bytes 68 | tf_op jit(solution)/shard_map/dynamic_slice | solution.py:128
  1.5 0.1 copy.71
  1.6 0.1 eq.56
  1.7 0.1 fusion.42
  1.7 0.7 %exp.10 = f32[16]{0:T(128)S(1)} exponential(f32[16]{0:T(128)} %param.25) | non-fusion elementwise | bytes 128 | tf_op jit(solution)/shard_map/exp | solution.py:26
  2.4 0.9 %fusion.19 = f32[4]{0:T(128)S(1)} fusion(bf16[4,2048]{1,0:T(4,128)(2,1)} %param.20), kind=kLoop, calls=%fused_computation.33 | loop fusion | flops 24572 | bytes 16400 | tf_op jit(solution)/shard_map/reduce_sum | solution.py:20
  3.3 0.7 %convert_element_type.68 = f32[2048]{0:T(1024)S(1)} convert(bf16[2048]{0:T(1024)(128)(2,1)} %param.21) | non-fusion elementwise | flops 2048 | bytes 12288 | tf_op jit(solution)/shard_map/convert_element_type | solution.py:21
  4.0 1.5 %convolution_convert_fusion.2 = bf16[4,256]{1,0:T(4,128)(2,1)S(1)} fusion(bf16[2048,256]{1,0:T(8,128)(2,1)} %param.22, bf16[4,2048]{1,0:T(4,128)(2,1)} %param.20, f32[2048]{0:T(1024)S(1)} %convert_element_type.68, f32[4]{0:T(128)S(1)} %add_rsqrt_fusion.1), kind=kOutput, calls=%fused_computation.14 | convolution fusion | flops 4228096 | bytes 1075216 | tf_op jit(solution)/shard_map/dot_general | solution.py:105
  5.5 0.1 reshape.72
  5.6 0.8 %cosine_multiply_fusion = (f32[16,64]{1,0:T(8,128)S(1)}, f32[16,64]{1,0:T(8,128)S(1)}, f32[16,64]{1,0:T(8,128)S(1)}, f32[16,64]{1,0:T(8,128)S(1)}) fusion(f32[16,64]{1,0:T(8,128)} %param.24, f32[16,64]{1,0:T(8,128)} %param.23, f32[16]{0:T(128)S(1)} %exp.10), kind=kLoop, calls=%fused_computation.52 | loop fusion | flops 17408 | bytes 24640 | tf_op jit(solution)/shard_map/mul | solution.py:30
  6.4 1.2 %fusion.2 = f32[4,16,64]{2,0,1:T(4,128)S(1)} fusion(f32[16,64,16]{1,2,0:T(8,128)} %param.26, f32[16,64,16]{1,2,0:T(8,128)} %param.27, f32[16,64]{1,0:T(8,128)S(1)} %get-tuple-element.21, f32[16,64]{1,0:T(8,128)S(1)} %get-tuple-element.20, f32[4,16,64]{2,1,0:T(8,128)} %param.32, f32[4,16,64]{2,1,0:T(8,128)} %param.31, f32[16,64]{1,0:T(8,128)S(1)} %get-tuple-element.22, ...), kind=kOutput, calls=%fused_computation.7 | convolution fusion | flops 851968 | bytes 198656 | tf_op jit(solution)/shard_map/sgp,gnp->sgn/dot_general | solution.py:61
  7.6 1.2 %fusion.3 = f32[4,16,64]{2,0,1:T(4,128)S(1)} fusion(f32[16,64,16]{1,2,0:T(8,128)} %param.27, f32[16,64,16]{1,2,0:T(8,128)} %param.26, f32[16,64]{1,0:T(8,128)S(1)} %get-tuple-element.21, f32[16,64]{1,0:T(8,128)S(1)} %get-tuple-element.20, f32[4,16,64]{2,1,0:T(8,128)} %param.32, f32[4,16,64]{2,1,0:T(8,128)} %param.31, f32[16,64]{1,0:T(8,128)S(1)} %get-tuple-element.22, ...), kind=kOutput, calls=%fused_computation.9 | convolution fusion | flops 851968 | bytes 198656 | tf_op jit(solution)/shard_map/sgp,gnp->sgn/dot_general | solution.py:60
  8.8 0.1 fusion.45
  8.9 0.1 fusion.43
  9.0 0.7 %convert_element_type.80 = f32[2048]{0:T(1024)S(1)} convert(bf16[2048]{0:T(1024)(128)(2,1)} %param.34) | non-fusion elementwise | flops 2048 | bytes 12288 | tf_op jit(solution)/shard_map/convert_element_type | solution.py:21
  9.7 1.2 %fusion.59 = f32[16,4,16]{2,1,0:T(4,128)S(1)} fusion(f32[4,16,64]{2,0,1:T(4,128)S(1)} %fusion.3, f32[16,16,64]{2,1,0:T(8,128)} %param.28), kind=kOutput, calls=%fused_computation.84 | convolution fusion | flops 786432 | bytes 86016 | tf_op jit(solution)/shard_map/sgn,gpn->sgp/dot_general | solution.py:64
  10.9 1.2 %fusion.1 = f32[4,16,16]{2,0,1:T(4,128)S(1)} fusion(f32[16,4,16]{2,1,0:T(4,128)S(1)} %fusion.59, f32[4,16,64]{2,0,1:T(4,128)S(1)} %fusion.2, f32[16,16,64]{2,1,0:T(8,128)} %param.29), kind=kOutput, calls=%fused_computation.5 | convolution fusion | flops 787456 | bytes 90112 | tf_op jit(solution)/shard_map/sgn,gpn->sgp/dot_general | solution.py:64
  12.1 0.1 reshape.73
  12.2 0.0 copy-done
  12.2 0.9 %convolution_bitcast_fusion = f32[1,4,2048]{2,1,0:T(4,128)S(1)} fusion(bf16[256,2048]{1,0:T(8,128)(2,1)S(1)} %copy-done, f32[4,256]{1,0:T(4,128)S(1)} %reshape.73, bf16[4,256]{1,0:T(4,128)(2,1)S(1)} %convolution_convert_fusion.2, f32[256]{0:T(256)} %param.30), kind=kOutput, calls=%fused_computation.3 | convolution fusion | flops 4206592 | bytes 1088512 | tf_op jit(solution)/shard_map/dot_general | solution.py:121
  13.2 6.5 %all-gather.1 = f32[4,4,2048]{2,1,0:T(4,128)S(1)} all-gather(f32[1,4,2048]{2,1,0:T(4,128)S(1)} %convolution_bitcast_fusion), channel_id=2, replica_groups=mesh['ep'=8,'tp'=4] {'tp'}, dimensions={0}, use_global_device_ids=true | all-gather | bytes 163840 | tf_op jit(solution)/shard_map/all_gather | solution.py:11
  19.7 0.9 %fusion.16 = (f32[4]{0:T(128)S(1)}, bf16[4,2048]{1,0:T(4,128)(2,1)S(1)}) fusion(f32[4,2048]{1,0:T(4,128)S(1)} %reduce_sum.50, bf16[4,2048]{1,0:T(4,128)(2,1)} %param.20), kind=kLoop, calls=%fused_computation.30 | loop fusion | flops 49148 | bytes 65552 | tf_op jit(solution)/shard_map/reduce_sum | solution.py:20
  20.6 0.8 %select_reduce_fusion.1 = (f32[4,8,2]{1,0,2:T(4,128)S(1)}, bf16[4,8,2]{1,0,2:T(4,128)(2,1)S(1)}) fusion(f32[4,2]{0,1:T(2,128)} %param.36, s32[4,2,8]{2,0,1:T(4,128)S(1)} %copy.73, pred[4,2,8]{2,0,1:T(4,128)(4,1)S(1)} %copy.74), kind=kLoop, calls=%fused_computation.46 | loop fusion | flops 640 | bytes 736 | tf_op jit(solution)/shard_map/reduce_sum | solution.py:78
  21.3 0.2 convolution_convert_fusion
  21.6 0.1 copy.75
  21.6 12.9 %all_to_all.10 = bf16[8,2,2048]{2,1,0:T(2,128)(2,1)S(1)} all-to-all(bf16[8,2,2048]{2,1,0:T(2,128)(2,1)S(1)} %copy.75), channel_id=1, replica_groups=mesh['ep'=8,'tp'=4] {'ep'}, dimensions={0} | all-to-all | bytes 131072 | tf_op jit(solution)/shard_map/all_to_all | solution.py:134
  34.5 4.6 %fusion.60 = f32[16,2048]{1,0:T(8,128)S(1)} fusion(bf16[16,2048]{1,0:T(8,128)(2,1)S(1)} %reshape.74, bf16[2048,2048]{1,0:T(8,128)(2,1)} %param.37), kind=kOutput, calls=%fused_computation.85 | convolution fusion | flops 134217728 | bytes 8585216 | tf_op jit(solution)/shard_map/dot_general | solution.py:138
  39.1 4.6 %fusion = bf16[16,2048]{1,0:T(8,128)(2,1)S(1)} fusion(bf16[16,2048]{1,0:T(8,128)(2,1)S(1)} %reshape.74, bf16[2048,2048]{1,0:T(8,128)(2,1)} %param.38, f32[16,2048]{1,0:T(8,128)S(1)} %fusion.60), kind=kOutput, calls=%fused_computation.2 | convolution fusion | flops 134414336 | bytes 8650752 | tf_op jit(solution)/shard_map/dot_general | solution.py:139
  43.7 5.8 %all_gather.11 = bf16[16,8192]{1,0:T(8,128)(2,1)S(1)} all-gather(bf16[16,2048]{1,0:T(8,128)(2,1)S(1)} %fusion), channel_id=1, replica_groups=mesh['ep'=8,'tp'=4] {'tp'}, dimensions={1}, use_global_device_ids=true | all-gather | bytes 327680 | tf_op jit(solution)/shard_map/all_gather | solution.py:143
  49.5 4.6 %convolution_convert_fusion.1 = bf16[16,512]{1,0:T(8,128)(2,1)S(1)} fusion(bf16[16,8192]{1,0:T(8,128)(2,1)S(1)} %all_gather.11, bf16[8192,512]{1,0:T(8,128)(2,1)} %param.39), kind=kOutput, calls=%fused_computation.10 | convolution fusion | flops 134225920 | bytes 8667136 | tf_op jit(solution)/shard_map/dot_general | solution.py:142
  54.0 0.6 reshape.75
  54.7 3.3 %all-to-all-start.1 = ((bf16[8,2,512]{2,1,0:T(2,128)(2,1)}), bf16[8,2,512]{2,1,0:T(2,128)(2,1)S(1)}, u32[]{:S(2)}, u32[]{:S(2)}) async-start(bf16[8,2,512]{2,1,0:T(2,128)(2,1)} %reshape.75), calls=%async_computation.1 | async-start | bytes 32768 | tf_op jit(solution)/shard_map/all_to_all | solution.py:148
  58.0 0.6 copy.77
  58.6 0.6 copy.78
  59.2 5.3 %all-to-all-done.1 = bf16[8,2,512]{2,1,0:T(2,128)(2,1)S(1)} async-done(((bf16[8,2,512]{2,1,0:T(2,128)(2,1)}), bf16[8,2,512]{2,1,0:T(2,128)(2,1)S(1)}, u32[]{:S(2)}, u32[]{:S(2)}) %all-to-all-start.1) | async-done | bytes 16416 | tf_op jit(solution)/shard_map/all_to_all | solution.py:148
  64.5 0.8 %fusion.5 = bf16[4,512]{1,0:T(4,128)(2,1)} fusion(bf16[8,2,512]{2,1,0:T(2,128)(2,1)S(1)} %all-to-all-done.1, f32[4,8,2]{1,0,2:T(4,128)S(1)} %get-tuple-element.15, bf16[4,2048]{1,0:T(4,128)(2,1)S(1)} %get-tuple-element.18, s32[]{:T(128)S(6)} %select_n.13), kind=kOutput, calls=%fused_computation.13 | convolution fusion | flops 399360 | bytes 24836 | tf_op jit(solution)/shard_map/xcs,xcd->sd/dot_general | solution.py:153
  (8 shorter events, 0.1 us)
Async XLA Ops:
  0.6 11.6 %copy-start = (bf16[256,2048]{1,0:T(8,128)(2,1)S(1)}, bf16[256,2048]{1,0:T(8,128)(2,1)}, u32[]{:S(2)}) copy-start(bf16[256,2048]{1,0:T(8,128)(2,1)} %param.33) | copy-start | bytes 3145732
  54.7 9.9 %all-to-all-start.1 = ((bf16[8,2,512]{2,1,0:T(2,128)(2,1)}), bf16[8,2,512]{2,1,0:T(2,128)(2,1)S(1)}, u32[]{:S(2)}, u32[]{:S(2)}) async-start(bf16[8,2,512]{2,1,0:T(2,128)(2,1)} %reshape.75), calls=%async_computation.1 | async-start | bytes 32768 | tf_op jit(solution)/shard_map/all_to_all | solution.py:148
